TPU v7x, 32 devices: a whole 2x2x4 slice. The times are simulated.
32 devices in a mesh: sp: 8 (over z, x), tp: 4 (over y, core).
Axes of the slice: x: 2, y: 2, z: 4, core: 2. Of those that a mesh axis runs over, the one named last changes fastest.
Arguments:
- stream: bfloat16 [2048, 2048], P(('sp', 'tp')), may hold values from -6 to 6
- query_a: bfloat16 [2048, 384], P('sp', 'tp'), may hold values from -400 to 400
- query_b: bfloat16 [2048, 640], P('sp', 'tp'), may hold values from -400 to 400
- latent: bfloat16 [2048, 256], P('sp'), may hold values from -6 to 6
- rotary_key: bfloat16 [2048, 32], P('sp'), may hold values from -6 to 6
- latent_gain: float32 [256], replicated, may hold values from 0.1 to 1.9
- key_gain_a: float32 [96], replicated, may hold values from 0.1 to 1.9
- key_gain_b: float32 [160], replicated, may hold values from 0.1 to 1.9
- w_key_a: bfloat16 [256, 256], P(None, 'tp'), may hold values from -0.375 to 0.375
- w_value_a: bfloat16 [256, 256], P(None, 'tp'), may hold values from -0.375 to 0.375
- w_key_b: bfloat16 [256, 512], P(None, 'tp'), may hold values from -0.375 to 0.375
- w_value_b: bfloat16 [256, 512], P(None, 'tp'), may hold values from -0.375 to 0.375
- w_out_a: bfloat16 [256, 2048], P('tp'), may hold values from -0.21875 to 0.21875
- w_out_b: bfloat16 [512, 2048], P('tp'), may hold values from -0.21875 to 0.21875
- norm_gain: float32 [2048], replicated, may hold values from 0.1 to 1.9
- w_up: bfloat16 [2048, 4096], P('sp', 'tp'), may hold values from -0.125 to 0.125
- w_down: bfloat16 [4096, 2048], P('tp', 'sp'), may hold values from -0.09375 to 0.09375
Outputs:
- result: bfloat16 [2048, 2048], P(('sp', 'tp'))
All inputs are finite; a program needn't handle non-finite values.
Results may differ from a plain program's by a relative error of at most 0.018.
The roundings to bfloat16 on the way count: a program that leaves them out, or rounds other values in their place, can miss the bound.
Values may be sent and summed in bfloat16 or wider, within the bound.
A program may use at most 128 MiB of HBM per device.

v0:
```python
import functools

import jax
import jax.numpy as jnp
import numpy as np
from jax import lax
from jax.experimental import pallas as pl
from jax.experimental.pallas import tpu as pltpu
from jax.sharding import PartitionSpec as P

NOPE_A = 64
V_A = 64
NOPE_B = 128
V_B = 128
ROPE = 32

EPSILON = 1e-06
THETA = 10000.0
F32 = jnp.float32
BF16 = jnp.bfloat16


def kernel(
    n, m,
    stream, q_a, q_b, packed, table, lat_gain, gain_a, gain_b,
    wk_a, wv_a, wk_b, wv_b, wo_a, wo_b, norm_gain, w_up, w_down,
    out,
    lat, key_a, key_b, val_a, val_b, att, rows, goa, gob,
    gup, gdown, x, hid, act, res, even, odd, sib, mid, part, land,
    lat_s, lat_r, latf_s, latf_r, oa_s, oa_r, ob_s, ob_r,
    up_s, up_r, dn_s, dn_r, at_s, at_r, x_s, x_r, rs_s, rs_r,
):
    s = lax.axis_index("sp")
    t = lax.axis_index("tp")
    core = t & 1
    length = q_a.shape[1]
    own = stream.shape[0]
    prow = packed.shape[0]
    half_rows = prow // 2
    depth_a = NOPE_A + ROPE
    depth_b = NOPE_B + ROPE
    heads_a = wk_a.shape[0] // NOPE_A
    heads_b = wk_b.shape[1] // NOPE_B
    hidden = gup.shape[2]
    wrows = w_up.shape[0]
    wcols = w_down.shape[1]
    width_a = heads_a * V_A
    width_b = heads_b * V_B
    start_b = att.shape[2] - width_b
    pending = []

    def copy(src, dst, ssem, rsem, sp, tp):
        return pltpu.make_async_remote_copy(
            src_ref=src, dst_ref=dst, send_sem=ssem, recv_sem=rsem,
            device_id={"sp": sp, "tp": tp}, device_id_type=pl.DeviceIdType.MESH,
        )

    def send(*args):
        c = copy(*args)
        c.start()
        pending.append(c)

    barrier = pltpu.get_barrier_semaphore()
    for k in range(1, n):
        pl.semaphore_signal(barrier, inc=1, device_id={"sp": s ^ k, "tp": t},
                            device_id_type=pl.DeviceIdType.MESH)
    for k in range(1, m):
        pl.semaphore_signal(barrier, inc=1, device_id={"sp": s, "tp": t ^ k},
                            device_id_type=pl.DeviceIdType.MESH)
    pl.semaphore_wait(barrier, n + m - 2)

    mine = pl.ds(pl.multiple_of(core * half_rows, 16), half_rows)
    other = pl.ds(pl.multiple_of((1 - core) * half_rows, 16), half_rows)
    for k in [1] + list(range(2, n, 2)):
        send(packed.at[mine], lat.at[k, mine], lat_s.at[k], lat_r.at[k], s ^ k, t)
    for k in (2, 1):
        send(wo_a, goa.at[k - 1], oa_s.at[k - 1], oa_r.at[k - 1], s, t ^ k)
        send(wo_b, gob.at[k - 1], ob_s.at[k - 1], ob_r.at[k - 1], s, t ^ k)

    def halves(target):
        return pl.ds(pl.multiple_of(((target // 2) % 2) * hidden, 128), hidden)

    for k in [1] + list(range(2, n, 2)):
        send(w_up.at[:, halves(s ^ k)], gup.at[k], up_s.at[k], up_r.at[k], s ^ k, t)
    for k in [1] + list(range(2, n, 2)):
        send(w_down.at[halves(s ^ k)], gdown.at[k], dn_s.at[k], dn_r.at[k], s ^ k, t)

    def make_block(k, source):
        start = pl.multiple_of(k * length, length)
        at = pl.ds(start, length)
        wide = source[0:length, :].astype(F32)
        normed = (wide * lax.rsqrt(jnp.mean(wide * wide, axis=-1, keepdims=True) + EPSILON)
                  * lat_gain[...]).astype(BF16)
        tail = source[length:prow, :].astype(F32)
        lanes = tail.shape[1] // ROPE
        rotary = jnp.concatenate([tail[:, i * ROPE:(i + 1) * ROPE] for i in range(lanes)], axis=0)
        squares = jnp.sum(rotary * rotary, axis=-1, keepdims=True)
        half = ROPE // 2
        turn = table[s ^ k]
        cosine = jnp.concatenate([turn[:, :half], turn[:, :half]], axis=-1)
        sine = jnp.concatenate([-turn[:, half:], turn[:, half:]], axis=-1)

        def turned(w):
            return lax.dot_general(normed, w[...], (((1,), (1,)), ((), ())),
                                   preferred_element_type=F32)

        def keys(flat, gain, nope, heads, dest):
            flat = flat.astype(BF16).astype(F32)
            for h in range(heads):
                piece = flat[:, h * nope:(h + 1) * nope]
                mean = (jnp.sum(piece * piece, axis=-1, keepdims=True) + squares) / (nope + ROPE)
                scale = lax.rsqrt(mean + EPSILON)
                dest[h, at, 0:nope] = (piece * scale * gain[:, 0:nope]).astype(BF16)
                last = rotary * scale * gain[:, nope:nope + ROPE]
                swapped = jnp.concatenate([last[:, half:], last[:, :half]], axis=-1)
                dest[h, at, nope:nope + ROPE] = (
                    last * cosine + swapped * sine).astype(BF16)

        keys(turned(wk_a), gain_a, NOPE_A, heads_a, key_a)
        keys(jnp.dot(normed, wk_b[...], preferred_element_type=F32), gain_b, NOPE_B, heads_b, key_b)
        val_a[at, :] = turned(wv_a).astype(BF16)
        val_b[at, :] = jnp.dot(normed, wv_b[...], preferred_element_type=F32).astype(BF16)

    make_block(0, packed)
    def arrived(k):
        copy(packed.at[mine], lat.at[k, mine], lat_s.at[k], lat_r.at[k], s ^ k, t).wait_recv()

    def to_sibling(k):
        send(lat.at[k, mine], lat.at[k, mine], latf_s.at[k], latf_r.at[k], s, t ^ 1)

    arrived(1)
    to_sibling(1)
    for k in range(2, n, 2):
        arrived(k)
        send(lat.at[k, mine], lat.at[k + 1, mine], lat_s.at[k + 1], lat_r.at[k + 1], s ^ 1, t)
        to_sibling(k)

    def weights_on(ref, ssem, rsem, k):
        copy(ref.at[k], ref.at[k], ssem.at[k], rsem.at[k], s ^ k, t).wait_recv()
        send(ref.at[k], ref.at[k + 1], ssem.at[k + 1], rsem.at[k + 1], s ^ 1, t)

    for k in range(3, n, 2):
        arrived(k)
        to_sibling(k)

    def one(k, carry):
        copy(lat.at[k, other], lat.at[k, other], latf_s.at[k], latf_r.at[k], s, t ^ 1).wait_recv()
        make_block(k, lat.at[k])
        return carry

    lax.fori_loop(1, n, one, 0)
    weights_on(gup, up_s, up_r, 2)
    weights_on(gup, up_s, up_r, 4)

    total = n * length
    block = min(total, 2048)
    number = total // block

    def attend(q, key, value, h, depth, width):
        query = q[h * depth:(h + 1) * depth, :].T

        def step(i, state):
            peak, sums, acc = state
            at = pl.ds(pl.multiple_of(i * block, block), block)
            score = lax.dot_general(query, key[h, at, :], (((1,), (1,)), ((), ())),
                                    preferred_element_type=F32) * depth ** (-0.5)
            new = jnp.maximum(peak, jnp.max(score, axis=-1, keepdims=True))
            shifted = jnp.exp(score - new)
            factor = jnp.exp(peak - new)
            sums = sums * factor + jnp.sum(shifted, axis=-1, keepdims=True)
            acc = acc * factor + jnp.dot(
                shifted.astype(BF16), value[at, h * width:(h + 1) * width],
                preferred_element_type=F32)
            return new, sums, acc

        state = (jnp.full((length, 1), -jnp.inf, F32), jnp.zeros((length, 1), F32),
                 jnp.zeros((length, width), F32))
        if number == 1:
            state = step(0, state)
        else:
            state = lax.fori_loop(0, number, step, state)
        return (state[2] / state[1]).astype(BF16)

    for h in range(heads_a):
        res_a = attend(q_a, key_a, val_a, h, depth_a, V_A)
        for j in range(m):
            att[j, :, h * V_A:(h + 1) * V_A] = res_a[j * own:(j + 1) * own]
    copy(wo_a, goa.at[1], oa_s.at[1], oa_r.at[1], s, t ^ 2).wait_recv()
    send(goa.at[1], goa.at[2], oa_s.at[2], oa_r.at[2], s, t ^ 1)
    copy(wo_b, gob.at[1], ob_s.at[1], ob_r.at[1], s, t ^ 2).wait_recv()
    send(gob.at[1], gob.at[2], ob_s.at[2], ob_r.at[2], s, t ^ 1)
    for h in range(heads_b):
        res_b = attend(q_b, key_b, val_b, h, depth_b, V_B)
        for j in range(m):
            att[j, :, start_b + h * V_B:start_b + (h + 1) * V_B] = res_b[j * own:(j + 1) * own]
    for k in range(1, m):
        send(att.at[t ^ k], rows.at[k], at_s.at[k], at_r.at[k], s, t ^ k)

    mixed = (jnp.dot(att[t, :, 0:width_a], wo_a[...], preferred_element_type=F32)
             + jnp.dot(att[t, :, start_b:], wo_b[...], preferred_element_type=F32))
    for k in range(1, m):
        copy(wo_a, goa.at[k - 1], oa_s.at[k - 1], oa_r.at[k - 1], s, t ^ 1) \
            .wait_recv() if k != 2 else None
        copy(wo_b, gob.at[k - 1], ob_s.at[k - 1], ob_r.at[k - 1], s, t ^ 1) \
            .wait_recv() if k != 2 else None
        copy(att.at[t ^ k], rows.at[k], at_s.at[k], at_r.at[k], s, t ^ k).wait_recv()
        mixed += jnp.dot(rows[k, :, 0:width_a], goa[k - 1], preferred_element_type=F32)
        mixed += jnp.dot(rows[k, :, start_b:], gob[k - 1], preferred_element_type=F32)
    residual = (stream[...].astype(F32) + mixed).astype(BF16)
    res[...] = residual
    wide = residual.astype(F32)
    x[0:own, :] = (wide * lax.rsqrt(jnp.mean(wide * wide, axis=-1, keepdims=True) + EPSILON)
                   * norm_gain[...]).astype(BF16)

    def peer(code):
        return (s ^ 2 if code & 4 else s), t ^ (code & 3)

    def slot(k):
        return x.at[pl.ds(k * own, own)]

    def xcopy(src, dst, code):
        return copy(slot(src), slot(dst), x_s.at[dst], x_r.at[dst], *peer(code))

    def xsend(src, dst, code):
        c = xcopy(src, dst, code)
        c.start()
        pending.append(c)

    for code in (2, 4, 1):
        xsend(0, code, code)
    for k in range(6, n, 2):
        weights_on(gup, up_s, up_r, k)
    weights_on(gdown, dn_s, dn_r, 2)
    xcopy(0, 2, 2).wait_recv()
    xcopy(0, 4, 4).wait_recv()
    diag = copy(
        x.at[pl.ds(pl.multiple_of((2 + 2 * core) * own, own), own)], slot(6),
        x_s.at[6], x_r.at[6], s ^ (2 - 2 * core), t ^ (2 * core))
    diag.start()
    pending.append(diag)
    xsend(2, 3, 1)
    xsend(4, 5, 1)
    diag.wait_recv()
    xsend(6, 7, 1)
    weights_on(gdown, dn_s, dn_r, 4)
    for k in (1, 3, 5, 7):
        xcopy(k - 1, k, 1).wait_recv()

    def columns(k, size):
        return pl.ds(pl.multiple_of((s ^ k) * size, 128), size)

    held = halves(s)
    hid[...] = jnp.dot(x[:, columns(0, wrows)], w_up[:, held], preferred_element_type=F32)

    def up(k):
        hid[...] += jnp.dot(x[:, columns(k, wrows)], gup[k], preferred_element_type=F32)

    def up_loop(i, carry):
        k = 2 * i
        copy(gup.at[k + 1], gup.at[k + 1], up_s.at[k + 1], up_r.at[k + 1], s ^ 1, t).wait_recv()
        up(k)
        up(k + 1)
        return carry

    copy(gup.at[1], gup.at[1], up_s.at[1], up_r.at[1], s ^ 1, t).wait_recv()
    up(1)
    lax.fori_loop(1, 3, up_loop, 0)
    lax.fori_loop(3, n // 2, up_loop, 0)
    for k in range(6, n, 2):
        weights_on(gdown, dn_s, dn_r, k)
    act[...] = jnp.square(jnp.maximum(hid[...], 0.0)).astype(BF16)

    group = n // 2

    def split(g, k, piece):
        at = pl.ds(pl.multiple_of(((s ^ k) % group) * wcols, 128), wcols)
        for i in range(4):
            even[g, i, :, at] = piece[2 * i * own:(2 * i + 1) * own]
            odd[g, i, :, at] = piece[(2 * i + 1) * own:(2 * i + 2) * own].astype(BF16)

    def down(g, k):
        split(g, k, jnp.dot(act[...], gdown[k], preferred_element_type=F32))

    def down_loop(g):
        def step(i, carry):
            k = 2 * i
            down(g, k)
            copy(gdown.at[k + 1], gdown.at[k + 1], dn_s.at[k + 1], dn_r.at[k + 1],
                 s ^ 1, t).wait_recv()
            down(g, k + 1)
            return carry
        return step

    def first(g):
        return copy(odd.at[g], sib.at[g], rs_s.at[4 * g], rs_r.at[4 * g], s, t ^ 1)

    def second(g):
        return copy(mid.at[g], land.at[g, 0], rs_s.at[4 * g + 1], rs_r.at[4 * g + 1],
                    s ^ (2 - 2 * core), t ^ (2 * core))

    def third(g):
        return copy(part.at[g, 0], land.at[g, 1], rs_s.at[4 * g + 2], rs_r.at[4 * g + 2],
                    s, t ^ 2)

    def fourth(g):
        return copy(part.at[g, 1], land.at[g, 2], rs_s.at[4 * g + 3], rs_r.at[4 * g + 3],
                    s ^ 2, t)

    def begin(c):
        c.start()
        pending.append(c)

    def diagonal(g):
        first(g).wait_recv()
        mid[g] = (even[g, 3] + sib[g, 3].astype(F32)).astype(BF16)
        begin(second(g))
        for i in range(3):
            even[g, i] += sib[g, i].astype(F32)

    def straight(g):
        second(g).wait_recv()
        even[g, 1 + core] += land[g, 0].astype(F32)
        for i in (1, 2):
            part[g, i - 1] = even[g, i].astype(BF16)
        begin(third(g))
        begin(fourth(g))

    def finish(g):
        third(g).wait_recv()
        fourth(g).wait_recv()
        summed = even[g, 0] + land[g, 1].astype(F32) + land[g, 2].astype(F32)
        base = (s // group) if g == 0 else 1 - s // group
        at = pl.ds(pl.multiple_of(base * (group * wcols), 128), group * wcols)
        out[:, at] = (res[:, at].astype(F32) + summed).astype(BF16)

    split(0, 0, jnp.dot(act[...], w_down[held, :], preferred_element_type=F32))
    copy(gdown.at[1], gdown.at[1], dn_s.at[1], dn_r.at[1], s ^ 1, t).wait_recv()
    down(0, 1)
    lax.fori_loop(1, group // 2, down_loop(0), 0)
    begin(first(0))
    diagonal(0)
    lax.fori_loop(group // 2, n // 2, down_loop(1), 0)
    straight(0)
    begin(first(1))
    diagonal(1)
    finish(0)
    straight(1)
    finish(1)
    for c in pending:
        c.wait_send()


def body(n, m, stream, query_a, query_b, latent, rotary_key, latent_gain, key_gain_a, key_gain_b,
         w_key_a, w_value_a, w_key_b, w_value_b, w_out_a, w_out_b, norm_gain, w_up, w_down):
    length, rank = latent.shape
    own, features = stream.shape
    lanes = rank // ROPE
    tail = rotary_key.reshape(lanes, length // lanes, ROPE).transpose(1, 0, 2)
    packed = jnp.concatenate([latent, tail.reshape(length // lanes, rank)], axis=0)
    half = ROPE // 2
    freqs = np.float32(THETA) ** (-np.arange(half, dtype=np.float32) / np.float32(half))
    angle = np.arange(n * length).astype(np.float32)[:, None] * freqs
    cosine, sine = np.cos(angle), np.sin(angle)
    table = jnp.asarray(np.concatenate([cosine, sine], axis=-1).reshape(n, length, ROPE))
    total = n * length
    heads_a = w_key_a.shape[1] // NOPE_A
    heads_b = w_key_b.shape[1] // NOPE_B
    width_a = -(-heads_a * V_A // 128) * 128
    width_b = heads_b * V_B
    hidden = w_up.shape[1] // 2
    V = pltpu.VMEM
    dma = lambda k: pltpu.SemaphoreType.DMA((k,))
    tokens = 2 * m * own
    scratch = [
        V((n,) + packed.shape, BF16),
        V((heads_a, total, NOPE_A + ROPE), BF16),
        V((heads_b, total, NOPE_B + ROPE), BF16),
        V((total, heads_a * V_A), BF16),
        V((total, heads_b * V_B), BF16),
        V((m, own, width_a + width_b), BF16),
        V((m, own, width_a + width_b), BF16),
        V((m - 1,) + w_out_a.shape, BF16),
        V((m - 1,) + w_out_b.shape, BF16),
        V((n, w_up.shape[0], hidden), BF16),
        V((n, hidden, w_down.shape[1]), BF16),
        V((tokens, features), BF16),
        V((tokens, hidden), F32),
        V((tokens, hidden), BF16),
        V((own, features), BF16),
        V((2, 4, own, features // 2), F32),
        V((2, 4, own, features // 2), BF16),
        V((2, 4, own, features // 2), BF16),
        V((2, own, features // 2), BF16),
        V((2, 2, own, features // 2), BF16),
        V((2, 3, own, features // 2), BF16),
    ]
    sizes = [n, n, n, n, 3, 3, 3, 3, n, n, n, n, m, m, 8, 8, 8, 8]
    scratch += [dma(k) for k in sizes]
    return pl.pallas_call(
        functools.partial(kernel, n, m),
        out_shape=jax.ShapeDtypeStruct((own, features), BF16),
        in_specs=[pl.BlockSpec(memory_space=V)] * 17,
        out_specs=pl.BlockSpec(memory_space=V),
        scratch_shapes=scratch,
        compiler_params=pltpu.CompilerParams(
            collective_id=0, has_side_effects=True, vmem_limit_bytes=67043328),
        name="layer",
    )(stream, query_a.T, query_b.T, packed, table, latent_gain[None], key_gain_a[None],
      key_gain_b[None], w_key_a.T, w_value_a.T, w_key_b, w_value_b, w_out_a, w_out_b,
      norm_gain[None], w_up, w_down)


def solution(mesh):
    n, m = mesh.shape["sp"], mesh.shape["tp"]
    in_specs = (
        P(("sp", "tp"), None),
        P("sp", "tp"),
        P("sp", "tp"),
        P("sp", None),
        P("sp", None),
        P(),
        P(),
        P(),
        P(None, "tp"),
        P(None, "tp"),
        P(None, "tp"),
        P(None, "tp"),
        P("tp", None),
        P("tp", None),
        P(),
        P("sp", "tp"),
        P("tp", "sp"),
    )
    out_specs = P(("sp", "tp"), None)
    return jax.shard_map(functools.partial(body, n, m), mesh=mesh, in_specs=in_specs,
                         out_specs=out_specs, check_vma=False)
```

profile of v0, /device:TPU:0, one launch (start us, length us, event | category | flops | bytes accessed | tf_op | source)
XLA Modules:
  0.0 88.4 jit_solution(14321895806806933897)
XLA Ops:
  0.0 0.0 copy-start
  0.0 0.9 reshape.6
  0.9 0.1 copy.19
  1.0 0.1 reshape.7
  1.1 0.0 copy-done
  1.1 0.7 pad_maximum_fusion.packed
  1.8 84.9 %layer.1 = bf16[64,2048]{1,0:T(8,128)(2,1)} custom-call(bf16[64,2048]{1,0:T(8,128)(2,1)} %stream.1, bf16[96,256]{1,0:T(8,128)(2,1)} %bitcast.13, bf16[160,256]{1,0:T(8,128)(2,1)} %bitcast.12, bf16[288,256]{1,0:T(8,128)(2,1)} %pad_maximum_fusion.packed, f32[8,256,32]{2,1,0:T(8,128)} %constant.2.clone.table, f32[1,256]{1,0:T(1,128)} %bitcast.17, ...), custom_call_target="tpu_custom_call" | custom-call | tf_op jit(solution)/shard_map/layer/pallas_call | solution.py:399
  86.7 1.7 %copy.21 = bf16[64,2048]{1,0:T(8,128)(2,1)} copy(bf16[64,2048]{1,0:T(8,128)(2,1)} %layer.1) | data formatting | bytes 524288
Async XLA Ops:
  0.0 1.1 %copy-start = (bf16[256,256]{1,0:T(8,128)(2,1)S(1)}, bf16[256,256]{1,0:T(8,128)(2,1)}, u32[]{:S(2)}) copy-start(bf16[256,256]{1,0:T(8,128)(2,1)} %param.21) | copy-start | bytes 393220
where the time goes:
time: 88.6 us; the launch traced here: 88.4 us
  Pallas kernels  84.9 us (96%)
  local copies, waits for them, and re-layouts  2.77 us (3%)
    pallas_call x1, Pallas kernels, body(): pl.pallas_call(functools.partial(kernel, n, m), out_shape=jax.ShapeDtypeS...  84.9 us

commit v1 on v0

v1 whole, which is shorter than its diff:
```python
import functools

import jax
import jax.numpy as jnp
import numpy as np
from jax import lax
from jax.experimental import pallas as pl
from jax.experimental.pallas import tpu as pltpu
from jax.sharding import PartitionSpec as P

NOPE_A = 64
V_A = 64
NOPE_B = 128
V_B = 128
ROPE = 32

EPSILON = 1e-06
THETA = 10000.0
F32 = jnp.float32
BF16 = jnp.bfloat16


def kernel(
    n, m,
    stream, q_a, q_b, latent, rotary_t, table_h, lat_gain, gain_a, gain_b,
    wk_a, wv_a, wk_b, wv_b, wo_a, wo_b, norm_gain, w_up, w_down,
    out,
    lat, key_a, key_b, val_a, val_b, att, rows, goa, gob,
    gup, gdown, x, hid, act, res, even, odd, sib, part, land, table,
    lat_s, lat_r, latz_s, latf_s, latf_r, oa_s, oa_r, ob_s, ob_r,
    up_s, up_r, dn_s, dn_r, at_s, at_r, x_s, x_r, rs_s, rs_r, loc,
):
    s = lax.axis_index("sp")
    t = lax.axis_index("tp")
    core = t & 1
    length = q_a.shape[1]
    own = stream.shape[0]
    prow = lat.shape[1]
    half_rows = prow // 2
    depth_a = NOPE_A + ROPE
    depth_b = NOPE_B + ROPE
    heads_a = wk_a.shape[0] // NOPE_A
    heads_b = wk_b.shape[1] // NOPE_B
    hidden = gup.shape[2]
    wrows = w_up.shape[0]
    wcols = w_down.shape[1]
    features = stream.shape[1]
    width_a = heads_a * V_A
    width_b = heads_b * V_B
    start_b = att.shape[2] - width_b
    quarter = n // 4
    per = n // 8
    zone = s // quarter
    inner = (zone ^ (zone // 2)) & 1
    near = list(range(2, 2 * quarter, 2))
    first_far = (2 + inner) * quarter
    last_far = (3 - inner) * quarter
    up_half = wrows // 2
    cuts = 2 if wcols % 256 == 0 else 1
    cut = wcols // cuts

    def every(start, fn):
        if per == 1:
            fn(start)
        else:
            def step(j, carry):
                fn(start + 2 * j)
                return carry
            lax.fori_loop(0, per, step, 0)

    def copy(src, dst, ssem, rsem, sp, tp):
        return pltpu.make_async_remote_copy(
            src_ref=src, dst_ref=dst, send_sem=ssem, recv_sem=rsem,
            device_id={"sp": sp, "tp": tp}, device_id_type=pl.DeviceIdType.MESH,
        )

    barrier = pltpu.get_barrier_semaphore()

    def greet(sp, tp):
        pl.semaphore_signal(barrier, inc=1, device_id={"sp": sp, "tp": tp},
                            device_id_type=pl.DeviceIdType.MESH)

    for k in range(1, n):
        greet(s ^ k, t)
    for k in range(1, m):
        greet(s, t ^ k)
    greet(s ^ 2, t ^ 2)

    def halves(target):
        return pl.ds(pl.multiple_of(((target // 2) % 2) * hidden, 128), hidden)

    locals_ = [
        pltpu.make_async_copy(latent, lat.at[0, pl.ds(0, length)], loc.at[0]),
        pltpu.make_async_copy(rotary_t, lat.at[0, pl.ds(length, prow - length)], loc.at[1]),
        pltpu.make_async_copy(table_h, table, loc.at[2]),
        pltpu.make_async_copy(w_up.at[:, halves(s)], gup.at[0], loc.at[3]),
        pltpu.make_async_copy(w_down.at[halves(s)], gdown.at[0], loc.at[4]),
    ]
    for c in locals_:
        c.start()
    locals_[0].wait()
    locals_[1].wait()
    pl.semaphore_wait(barrier, n + m - 1)

    mine = pl.ds(pl.multiple_of(core * half_rows, 16), half_rows)
    other = pl.ds(pl.multiple_of((1 - core) * half_rows, 16), half_rows)

    def lat_direct(k):
        return copy(lat.at[0, mine], lat.at[k, mine], lat_s.at[k], lat_r.at[k], s ^ k, t)

    def lat_across(k):
        return copy(lat.at[k, mine], lat.at[k + 1, mine], lat_s.at[k + 1], lat_r.at[k + 1], s ^ 1, t)

    def lat_along(k):
        j = k ^ quarter
        return copy(lat.at[k, mine], lat.at[j, mine], latz_s.at[k], lat_r.at[j], s ^ quarter, t)

    def lat_sibling(k):
        return copy(lat.at[k, mine], lat.at[k, mine], latf_s.at[k], latf_r.at[k], s, t ^ 1)

    def up_piece(k, r):
        at = pl.ds(r * up_half, up_half)
        return copy(w_up.at[at, halves(s ^ k)], gup.at[k, at], up_s.at[2 * k + r],
                    up_r.at[2 * k + r], s ^ k, t)

    def up_across(k, r):
        at = pl.ds(r * up_half, up_half)
        return copy(gup.at[k, at], gup.at[k + 1, at], up_s.at[2 * k + 2 + r],
                    up_r.at[2 * k + 2 + r], s ^ 1, t)

    def down_piece(k, h):
        at = pl.ds(h * cut, cut)
        return copy(w_down.at[halves(s ^ k), at], gdown.at[k, :, at], dn_s.at[2 * k + h],
                    dn_r.at[2 * k + h], s ^ k, t)

    def down_across(k, h):
        at = pl.ds(h * cut, cut)
        return copy(gdown.at[k, :, at], gdown.at[k + 1, :, at], dn_s.at[2 * k + 2 + h],
                    dn_r.at[2 * k + 2 + h], s ^ 1, t)

    def up_send(k):
        for r in range(2):
            up_piece(k, r).start()

    def down_send(k):
        for h in range(cuts):
            down_piece(k, h).start()

    def up_on(k):
        for r in range(2):
            up_piece(k, r).wait_recv()
            up_across(k, r).start()

    def up_arrived(k):
        for r in range(2):
            up_piece(k, r).wait_recv()

    def down_on(k, h):
        down_piece(k, h).wait_recv()
        down_across(k, h).start()

    def downs_on(k):
        for h in range(cuts):
            down_on(k, h)

    def outer_only(fn):
        pl.when(inner == 0)(fn)

    def inner_only(fn):
        pl.when(inner == 1)(fn)

    lat_direct(1).start()
    for k in near:
        lat_direct(k).start()
    every(first_far, lambda k: lat_direct(k).start())
    up_piece(1, 0).start()

    def out_a(k, slot):
        return copy(wo_a, goa.at[slot], oa_s.at[slot], oa_r.at[slot], s, t ^ k)

    def out_b(k, slot):
        return copy(wo_b, gob.at[slot], ob_s.at[slot], ob_r.at[slot], s, t ^ k)

    for k in (2, 1):
        out_a(k, k - 1).start()
        out_b(k, k - 1).start()

    @inner_only
    def _():
        every(last_far, up_send)
        every(first_far, up_send)
        every(first_far, down_send)
        every(last_far, down_send)

    @outer_only
    def _():
        for k in near:
            up_send(k)
        every(first_far, up_send)
        every(last_far, up_send)

    def make_block(k):
        source = lat.at[k]
        at = pl.ds(pl.multiple_of(k * length, length), length)
        wide = source[0:length, :].astype(F32)
        normed = (wide * lax.rsqrt(jnp.mean(wide * wide, axis=-1, keepdims=True) + EPSILON)
                  * lat_gain[...]).astype(BF16)
        rotary = source[length:prow, :].astype(F32).T
        squares = jnp.sum(rotary * rotary, axis=-1, keepdims=True)
        half = ROPE // 2
        turn = table[s ^ k]
        cosine = jnp.concatenate([turn[:, :half], turn[:, :half]], axis=-1)
        sine = jnp.concatenate([-turn[:, half:], turn[:, half:]], axis=-1)

        def turned(w):
            return lax.dot_general(normed, w[...], (((1,), (1,)), ((), ())),
                                   preferred_element_type=F32)

        def keys(flat, gain, nope, heads, dest):
            flat = flat.astype(BF16).astype(F32)
            for h in range(heads):
                piece = flat[:, h * nope:(h + 1) * nope]
                mean = (jnp.sum(piece * piece, axis=-1, keepdims=True) + squares) / (nope + ROPE)
                scale = lax.rsqrt(mean + EPSILON)
                dest[h, at, 0:nope] = (piece * scale * gain[:, 0:nope]).astype(BF16)
                last = rotary * scale * gain[:, nope:nope + ROPE]
                swapped = jnp.concatenate([last[:, half:], last[:, :half]], axis=-1)
                dest[h, at, nope:nope + ROPE] = (
                    last * cosine + swapped * sine).astype(BF16)

        keys(turned(wk_a), gain_a, NOPE_A, heads_a, key_a)
        keys(jnp.dot(normed, wk_b[...], preferred_element_type=F32), gain_b, NOPE_B, heads_b, key_b)
        val_a[at, :] = turned(wv_a).astype(BF16)
        val_b[at, :] = jnp.dot(normed, wv_b[...], preferred_element_type=F32).astype(BF16)

    locals_[2].wait()
    make_block(0)

    def arrived(k):
        lat_direct(k).wait_recv()

    def joined(k):
        copy(lat.at[k, other], lat.at[k, other], latf_s.at[k], latf_r.at[k], s, t ^ 1).wait_recv()
        make_block(k)

    def passed(k):
        arrived(k)
        lat_across(k).start()
        lat_sibling(k).start()

    def relayed(k):
        arrived(k)
        inner_only(lambda: lat_along(k).start())
        lat_across(k).start()
        lat_sibling(k).start()

    def taken(k):
        arrived(k)
        lat_sibling(k).start()

    taken(1)
    for k in near:
        passed(k)
    every(first_far, relayed)
    joined(1)
    every(last_far, relayed)

    @inner_only
    def _():
        for k in near:
            up_send(k)
        for k in near:
            down_send(k)

    up_piece(1, 1).start()
    down_send(1)
    for k in near:
        joined(k)
    for k in near:
        taken(k + 1)
    every(first_far, joined)
    every(first_far + 1, taken)
    every(last_far, joined)
    every(last_far + 1, taken)
    for k in near:
        joined(k + 1)
    every(first_far + 1, joined)
    every(last_far + 1, joined)

    total = n * length
    block = min(total, 2048)
    number = total // block

    def attend(q, key, value, h, depth, width):
        query = q[h * depth:(h + 1) * depth, :].T

        def step(i, state):
            peak, sums, acc = state
            at = pl.ds(pl.multiple_of(i * block, block), block)
            score = lax.dot_general(query, key[h, at, :], (((1,), (1,)), ((), ())),
                                    preferred_element_type=F32) * depth ** (-0.5)
            new = jnp.maximum(peak, jnp.max(score, axis=-1, keepdims=True))
            shifted = jnp.exp(score - new)
            factor = jnp.exp(peak - new)
            sums = sums * factor + jnp.sum(shifted, axis=-1, keepdims=True)
            acc = acc * factor + jnp.dot(
                shifted.astype(BF16), value[at, h * width:(h + 1) * width],
                preferred_element_type=F32)
            return new, sums, acc

        state = (jnp.full((length, 1), -jnp.inf, F32), jnp.zeros((length, 1), F32),
                 jnp.zeros((length, width), F32))
        if number == 1:
            state = step(0, state)
        else:
            state = lax.fori_loop(0, number, step, state)
        return (state[2] / state[1]).astype(BF16)

    for h in range(heads_a):
        res_a = attend(q_a, key_a, val_a, h, depth_a, V_A)
        for j in range(m):
            att[j, :, h * V_A:(h + 1) * V_A] = res_a[j * own:(j + 1) * own]
    for h in range(heads_b):
        res_b = attend(q_b, key_b, val_b, h, depth_b, V_B)
        for j in range(m):
            att[j, :, start_b + h * V_B:start_b + (h + 1) * V_B] = res_b[j * own:(j + 1) * own]

    def row_copy(k):
        return copy(att.at[t ^ k], rows.at[k], at_s.at[k], at_r.at[k], s, t ^ k)

    for k in (2, 3, 1):
        row_copy(k).start()

    def out_on_a():
        return copy(goa.at[1], goa.at[2], oa_s.at[2], oa_r.at[2], s, t ^ 1)

    def out_on_b():
        return copy(gob.at[1], gob.at[2], ob_s.at[2], ob_r.at[2], s, t ^ 1)

    def project(k, slot):
        return (jnp.dot(rows[k, :, 0:width_a], goa[slot], preferred_element_type=F32)
                + jnp.dot(rows[k, :, start_b:], gob[slot], preferred_element_type=F32))

    mixed = (jnp.dot(att[t, :, 0:width_a], wo_a[...], preferred_element_type=F32)
             + jnp.dot(att[t, :, start_b:], wo_b[...], preferred_element_type=F32))
    out_a(1, 0).wait_recv()
    out_b(1, 0).wait_recv()
    row_copy(1).wait_recv()
    mixed += project(1, 0)
    out_a(2, 1).wait_recv()
    out_on_a().start()
    out_b(2, 1).wait_recv()
    out_on_b().start()
    row_copy(2).wait_recv()
    mixed += project(2, 1)
    out_on_a().wait_recv()
    out_on_b().wait_recv()
    row_copy(3).wait_recv()
    mixed += project(3, 2)
    residual = (stream[...].astype(F32) + mixed).astype(BF16)
    res[...] = residual
    wide = residual.astype(F32)
    x[0:own, :] = (wide * lax.rsqrt(jnp.mean(wide * wide, axis=-1, keepdims=True) + EPSILON)
                   * norm_gain[...]).astype(BF16)

    def peer(code):
        return (s ^ 2 if code & 4 else s), t ^ (code & 3)

    bit = own // 2

    class xcopy:
        def __init__(self, src, dst, code):
            self.parts = [
                copy(x.at[pl.ds(src * own + i * bit, bit)], x.at[pl.ds(dst * own + i * bit, bit)],
                     x_s.at[2 * dst + i], x_r.at[2 * dst + i], *peer(code)) for i in range(2)]

        def start(self):
            for c in self.parts:
                c.start()

        def wait_recv(self):
            for c in self.parts:
                c.wait_recv()

        def wait_send(self):
            for c in self.parts:
                c.wait_send()

    def xrelay():
        for i in range(2):
            xcopy(0, 4, 4).parts[i].wait_recv()
            xcopy(4, 6, 2).parts[i].start()
            xcopy(4, 5, 1).parts[i].start()

    xcopy(0, 4, 4).start()
    xcopy(0, 2, 2).start()
    xcopy(0, 1, 1).start()

    @outer_only
    def _():
        for k in near:
            down_send(k)
        every(first_far, lambda k: down_piece(k, 0).start())
        every(last_far, lambda k: down_piece(k, 0).start())
        if cuts > 1:
            every(first_far, lambda k: down_piece(k, 1).start())
            every(last_far, lambda k: down_piece(k, 1).start())

    for k in near:
        up_on(k)
    every(2 * quarter, up_on)
    xcopy(0, 2, 2).wait_recv()
    xcopy(2, 3, 1).start()
    every(3 * quarter, up_on)
    xrelay()

    @outer_only
    def _():
        for k in near:
            downs_on(k)

    xcopy(4, 6, 2).wait_recv()
    xcopy(6, 7, 1).start()

    @inner_only
    def _():
        for k in near:
            downs_on(k)
        every(3 * quarter, downs_on)

    def columns(k, size):
        return pl.ds(pl.multiple_of((s ^ k) * size, 128), size)

    def up(k):
        hid[...] += jnp.dot(x[:, columns(k, wrows)], gup[k], preferred_element_type=F32)

    def up_pair(k):
        up(k)
        up_arrived(k + 1)
        up(k + 1)

    for k in (1, 3, 5, 7):
        xcopy(k - 1, k, 1).wait_recv()
    locals_[3].wait()
    locals_[4].wait()
    hid[...] = jnp.dot(x[:, columns(0, wrows)], gup[0], preferred_element_type=F32)
    up_arrived(1)
    up(1)
    for k in near:
        up_pair(k)
    every(2 * quarter, up_pair)
    every(3 * quarter, up_pair)
    act[...] = jnp.square(jnp.maximum(hid[...], 0.0)).astype(BF16)

    def down(unit, k, h, width):
        base = ((s ^ k) % quarter) * width
        at = pl.ds(pl.multiple_of(base, 128), width)
        first = 0 if h is None else h * cut
        piece = jnp.dot(act[...], gdown[k, :, first:first + width], preferred_element_type=F32)
        for i in range(4):
            even[unit, i, :, at] = piece[2 * i * own:(2 * i + 1) * own]
            odd[unit, i, :, at] = piece[(2 * i + 1) * own:(2 * i + 2) * own].astype(BF16)

    def down_arrived(k):
        for h in range(cuts):
            down_piece(k, h).wait_recv()

    def down_pair(unit):
        def fn(k):
            down(unit, k, None, wcols)
            down_arrived(k + 1)
            down(unit, k + 1, None, wcols)
        return fn

    full = quarter * wcols
    mine_u = zone & 1
    next_u = 1 - mine_u
    places = ((2, s, t ^ 2), (4, s ^ 2, t), (6, s ^ 2, t ^ 2))

    def share(unit, width):
        return copy(odd.at[unit, :, :, 0:width], sib.at[unit, :, :, 0:width],
                    rs_s.at[4 * unit], rs_r.at[4 * unit], s, t ^ 1)

    def deliver(unit, width, i):
        _, sp, tp = places[i]
        return copy(part.at[unit, i, :, 0:width], land.at[unit, i, :, 0:width],
                    rs_s.at[4 * unit + 1 + i], rs_r.at[4 * unit + 1 + i], sp, tp)

    def scatter(unit, width):
        share(unit, width).wait_recv()
        for i in (2, 1, 0):
            part[unit, i, :, 0:width] = (even[unit, i + 1, :, 0:width]
                                         + sib[unit, i + 1, :, 0:width].astype(F32)).astype(BF16)
            deliver(unit, width, i).start()
        even[unit, 0, :, 0:width] += sib[unit, 0, :, 0:width].astype(F32)

    def finish(unit, width, group, h):
        for i in range(3):
            deliver(unit, width, i).wait_recv()
        base = (zone ^ group) * full
        spans = [(0, 0, full)] if h is None or cuts == 1 else [
            (j * cut, j * wcols + h * cut, cut) for j in range(quarter)]
        for lo, to, size in spans:
            at = pl.ds(pl.multiple_of(base + to, 128), size)
            out[:, at] = (res[:, at].astype(F32) + even[unit, 0, :, lo:lo + size]
                          + land[unit, 0, :, lo:lo + size].astype(F32)
                          + land[unit, 1, :, lo:lo + size].astype(F32)
                          + land[unit, 2, :, lo:lo + size].astype(F32)).astype(BF16)

    narrow = quarter * cut

    def far_unit(group, h):
        return 2 + cuts * ((zone ^ group) & 1) + h

    def far(group, h):
        start = group * quarter
        unit = far_unit(group, h)
        every(start, lambda k: down(unit, k, h, cut))
        every(start + 1, lambda k: down_piece(k, h).wait_recv())
        every(start + 1, lambda k: down(unit, k, h, cut))
        share(unit, narrow).start()

    def far_on(h):
        every(2 * quarter, lambda k: down_on(k, h))

    down(mine_u, 0, None, wcols)
    down_arrived(1)
    down(mine_u, 1, None, wcols)
    for k in near:
        if k < quarter:
            down_pair(mine_u)(k)
    share(mine_u, full).start()
    outer_only(lambda: every(3 * quarter, downs_on))
    for k in near:
        if k >= quarter:
            down_pair(next_u)(k)
    share(next_u, full).start()
    scatter(mine_u, full)
    far_on(0)
    for h in range(cuts):
        far(3, h)
        if h == 0:
            scatter(next_u, full)
        else:
            scatter(far_unit(3, h - 1), narrow)
    for h in range(1, cuts):
        far_on(h)
    for h in range(cuts):
        far(2, h)
        if h == 0:
            scatter(far_unit(3, cuts - 1), narrow)
            finish(mine_u, full, 0, None)
            finish(next_u, full, 1, None)
        else:
            scatter(far_unit(2, h - 1), narrow)
    scatter(far_unit(2, cuts - 1), narrow)
    for h in range(cuts):
        finish(far_unit(3, h), narrow, 3, h)
    for h in range(cuts):
        finish(far_unit(2, h), narrow, 2, h)

    lat_direct(1).wait_send()
    up_piece(1, 0).wait_send()
    up_piece(1, 1).wait_send()

    def sent(k):
        lat_across(k).wait_send()
        for r in range(2):
            up_piece(k, r).wait_send()
            up_across(k, r).wait_send()
        for h in range(cuts):
            down_piece(k, h).wait_send()
            down_across(k, h).wait_send()

    for k in near:
        lat_direct(k).wait_send()
        sent(k)
    every(first_far, lambda k: lat_direct(k).wait_send())
    every(first_far, sent)
    every(last_far, sent)

    @inner_only
    def _():
        every(first_far, lambda k: lat_along(k).wait_send())
        every(last_far, lambda k: lat_along(k).wait_send())

    def settled(k, carry):
        lat_sibling(k).wait_send()
        return carry

    lax.fori_loop(1, n, settled, 0)
    for h in range(cuts):
        down_piece(1, h).wait_send()
    for k in (1, 2):
        out_a(k, k - 1).wait_send()
        out_b(k, k - 1).wait_send()
    out_on_a().wait_send()
    out_on_b().wait_send()
    for k in range(1, m):
        row_copy(k).wait_send()
    for src, dst, code in ((0, 4, 4), (0, 2, 2), (0, 1, 1), (2, 3, 1), (4, 6, 2), (4, 5, 1), (6, 7, 1)):
        xcopy(src, dst, code).wait_send()
    units = [(0, full), (1, full)] + [(2 + i, narrow) for i in range(2 * cuts)]
    for unit, width in units:
        share(unit, width).wait_send()
        for i in range(3):
            deliver(unit, width, i).wait_send()


def body(n, m, stream, query_a, query_b, latent, rotary_key, latent_gain, key_gain_a, key_gain_b,
         w_key_a, w_value_a, w_key_b, w_value_b, w_out_a, w_out_b, norm_gain, w_up, w_down):
    length, rank = latent.shape
    own, features = stream.shape
    half = ROPE // 2
    freqs = np.float32(THETA) ** (-np.arange(half, dtype=np.float32) / np.float32(half))
    angle = np.arange(n * length).astype(np.float32)[:, None] * freqs
    cosine, sine = np.cos(angle), np.sin(angle)
    table = jnp.asarray(np.concatenate([cosine, sine], axis=-1).reshape(n, length, ROPE))
    total = n * length
    heads_a = w_key_a.shape[1] // NOPE_A
    heads_b = w_key_b.shape[1] // NOPE_B
    width_a = -(-heads_a * V_A // 128) * 128
    width_b = heads_b * V_B
    hidden = w_up.shape[1] // 2
    V = pltpu.VMEM
    dma = lambda k: pltpu.SemaphoreType.DMA((k,))
    tokens = 2 * m * own
    group = features // 4
    units = 6 if w_down.shape[1] % 256 == 0 else 4
    scratch = [
        V((n, length + ROPE, rank), BF16),
        V((heads_a, total, NOPE_A + ROPE), BF16),
        V((heads_b, total, NOPE_B + ROPE), BF16),
        V((total, heads_a * V_A), BF16),
        V((total, heads_b * V_B), BF16),
        V((m, own, width_a + width_b), BF16),
        V((m, own, width_a + width_b), BF16),
        V((m - 1,) + w_out_a.shape, BF16),
        V((m - 1,) + w_out_b.shape, BF16),
        V((n, w_up.shape[0], hidden), BF16),
        V((n, hidden, w_down.shape[1]), BF16),
        V((tokens, features), BF16),
        V((tokens, hidden), F32),
        V((tokens, hidden), BF16),
        V((own, features), BF16),
        V((units, 4, own, group), F32),
        V((units, 4, own, group), BF16),
        V((units, 4, own, group), BF16),
        V((units, 3, own, group), BF16),
        V((units, 3, own, group), BF16),
        V(table.shape, F32),
    ]
    sizes = [n, n, n, n, n, 3, 3, 3, 3, 2 * n, 2 * n, 2 * n, 2 * n, m, m, 16, 16, 24, 24, 5]
    scratch += [dma(k) for k in sizes]
    vmem = pl.BlockSpec(memory_space=V)
    hbm = pl.BlockSpec(memory_space=pl.ANY)
    return pl.pallas_call(
        functools.partial(kernel, n, m),
        out_shape=jax.ShapeDtypeStruct((own, features), BF16),
        in_specs=[vmem, vmem, vmem, hbm, hbm, hbm, vmem, vmem, vmem, vmem, vmem, vmem, vmem,
                  vmem, vmem, vmem, hbm, hbm],
        out_specs=vmem,
        scratch_shapes=scratch,
        compiler_params=pltpu.CompilerParams(
            collective_id=0, has_side_effects=True, vmem_limit_bytes=67043328),
        name="layer",
    )(stream, query_a.T, query_b.T, latent, rotary_key.T, table, latent_gain[None], key_gain_a[None],
      key_gain_b[None], w_key_a.T, w_value_a.T, w_key_b, w_value_b, w_out_a, w_out_b,
      norm_gain[None], w_up, w_down)


def solution(mesh):
    n, m = mesh.shape["sp"], mesh.shape["tp"]
    in_specs = (
        P(("sp", "tp"), None),
        P("sp", "tp"),
        P("sp", "tp"),
        P("sp", None),
        P("sp", None),
        P(),
        P(),
        P(),
        P(None, "tp"),
        P(None, "tp"),
        P(None, "tp"),
        P(None, "tp"),
        P("tp", None),
        P("tp", None),
        P(),
        P("sp", "tp"),
        P("tp", "sp"),
    )
    out_specs = P(("sp", "tp"), None)
    return jax.shard_map(functools.partial(body, n, m), mesh=mesh, in_specs=in_specs,
                         out_specs=out_specs, check_vma=False)
```

time: 88.6 us -> 78.1 us (0.88)
  Pallas kernels: 84.9 us -> 76.3 us
  local copies, waits for them, and re-layouts: 2.77 us -> 1.67 us
    pallas_call x1, Pallas kernels: 84.9 us -> 76.3 us  [body(): pl.pallas_call(functools.partial(kernel, n, m), out_shape=jax.ShapeDtypeS...]
    reshape x3 -> x0, local copies, waits for them, and re-layouts: 1.09 us -> none  [the longest x2 0.99 us: body(): tail = rotary_key.reshape(lanes, length // lanes, ROPE).transpose(1, 0, 2)]
where the time goes in v1:
time: 78.1 us; the launch traced here: 77.9 us
  Pallas kernels  76.3 us (98%)
  local copies, waits for them, and re-layouts  1.67 us (2%)
    pallas_call x1, Pallas kernels, body(): pl.pallas_call(functools.partial(kernel, n, m), out_shape=jax.ShapeDtypeS...  76.3 us
    unnamed x1, local copies, waits for them, and re-layouts  1.67 us

profile of v1, /device:TPU:0, one launch (start us, length us, event | category | flops | bytes accessed | tf_op | source)
XLA Modules:
  0.0 77.9 jit_solution(5215397429323994802)
XLA Ops:
  0.0 76.3 %layer.1 = bf16[64,2048]{1,0:T(8,128)(2,1)} custom-call(bf16[64,2048]{1,0:T(8,128)(2,1)} %stream.1, bf16[96,256]{1,0:T(8,128)(2,1)} %bitcast.10, bf16[160,256]{1,0:T(8,128)(2,1)} %bitcast.9, bf16[256,256]{1,0:T(8,128)(2,1)} %latent.1, bf16[32,256]{1,0:T(8,128)(2,1)} %bitcast.13, f32[8,256,32]{2,1,0:T(8,128)} %constant.2.clone.table_h, f32[1,256]{1,0:T(1,128)} %bitcast.15, ...), custom_call_target="tpu_custom_call" | custom-call | tf_op jit(solution)/shard_map/layer/pallas_call | solution.py:657
  76.3 1.7 %copy.20 = bf16[64,2048]{1,0:T(8,128)(2,1)} copy(bf16[64,2048]{1,0:T(8,128)(2,1)} %layer.1) | data formatting | bytes 524288

commit v2 on v1

--- a/solution.py
+++ b/solution.py
@@ -22,12 +22,13 @@
 
 def kernel(
     n, m,
-    stream, q_a, q_b, latent, rotary_t, table_h, lat_gain, gain_a, gain_b,
-    wk_a, wv_a, wk_b, wv_b, wo_a, wo_b, norm_gain, w_up, w_down,
+    stream_h, q_a_h, q_b_h, latent, rotary_t, table_h, lat_gain_h, gain_a_h, gain_b_h,
+    wk_a_h, wv_a_h, wk_b_h, wv_b_h, wo_a_h, wo_b_h, norm_gain_h, w_up, w_down,
     out,
     lat, key_a, key_b, val_a, val_b, att, rows, goa, gob,
     gup, gdown, x, hid, act, res, even, odd, sib, part, land, table,
-    lat_s, lat_r, latz_s, latf_s, latf_r, oa_s, oa_r, ob_s, ob_r,
+    stream, q_a, q_b, lat_gain, gain_a, gain_b, wk_a, wv_a, wk_b, wv_b, wo_a, wo_b, norm_gain,
+    lat_s, lat_r, latf_s, latf_r, oa_s, oa_r, ob_s, ob_r,
     up_s, up_r, dn_s, dn_r, at_s, at_r, x_s, x_r, rs_s, rs_r, loc,
 ):
     s = lax.axis_index("sp")
@@ -96,7 +97,13 @@
         pltpu.make_async_copy(w_up.at[:, halves(s)], gup.at[0], loc.at[3]),
         pltpu.make_async_copy(w_down.at[halves(s)], gdown.at[0], loc.at[4]),
     ]
-    for c in locals_:
+    early = [pltpu.make_async_copy(a, b, loc.at[5 + i]) for i, (a, b) in enumerate((
+        (lat_gain_h, lat_gain), (gain_a_h, gain_a), (gain_b_h, gain_b), (wk_a_h, wk_a),
+        (wv_a_h, wv_a), (wk_b_h, wk_b), (wv_b_h, wv_b)))]
+    later = [pltpu.make_async_copy(a, b, loc.at[12 + i]) for i, (a, b) in enumerate((
+        (q_a_h, q_a), (q_b_h, q_b), (wo_a_h, wo_a), (wo_b_h, wo_b), (stream_h, stream),
+        (norm_gain_h, norm_gain)))]
+    for c in locals_[:2] + early + locals_[2:] + later:
         c.start()
     locals_[0].wait()
     locals_[1].wait()
@@ -111,10 +118,6 @@
     def lat_across(k):
         return copy(lat.at[k, mine], lat.at[k + 1, mine], lat_s.at[k + 1], lat_r.at[k + 1], s ^ 1, t)
 
-    def lat_along(k):
-        j = k ^ quarter
-        return copy(lat.at[k, mine], lat.at[j, mine], latz_s.at[k], lat_r.at[j], s ^ quarter, t)
-
     def lat_sibling(k):
         return copy(lat.at[k, mine], lat.at[k, mine], latf_s.at[k], latf_r.at[k], s, t ^ 1)
 
@@ -173,13 +176,14 @@
     for k in near:
         lat_direct(k).start()
     every(first_far, lambda k: lat_direct(k).start())
+    every(last_far, lambda k: lat_direct(k).start())
     up_piece(1, 0).start()
 
     def out_a(k, slot):
-        return copy(wo_a, goa.at[slot], oa_s.at[slot], oa_r.at[slot], s, t ^ k)
+        return copy(wo_a_h, goa.at[slot], oa_s.at[slot], oa_r.at[slot], s, t ^ k)
 
     def out_b(k, slot):
-        return copy(wo_b, gob.at[slot], ob_s.at[slot], ob_r.at[slot], s, t ^ k)
+        return copy(wo_b_h, gob.at[slot], ob_s.at[slot], ob_r.at[slot], s, t ^ k)
 
     for k in (2, 1):
         out_a(k, k - 1).start()
@@ -191,6 +195,8 @@
         every(first_far, up_send)
         every(first_far, down_send)
         every(last_far, down_send)
+        for k in near:
+            up_send(k)
 
     @outer_only
     def _():
@@ -234,6 +240,8 @@
         val_b[at, :] = jnp.dot(normed, wv_b[...], preferred_element_type=F32).astype(BF16)
 
     locals_[2].wait()
+    for c in early:
+        c.wait()
     make_block(0)
 
     def arrived(k):
@@ -248,12 +256,6 @@
         lat_across(k).start()
         lat_sibling(k).start()
 
-    def relayed(k):
-        arrived(k)
-        inner_only(lambda: lat_along(k).start())
-        lat_across(k).start()
-        lat_sibling(k).start()
-
     def taken(k):
         arrived(k)
         lat_sibling(k).start()
@@ -261,17 +263,9 @@
     taken(1)
     for k in near:
         passed(k)
-    every(first_far, relayed)
+    every(first_far, passed)
     joined(1)
-    every(last_far, relayed)
-
-    @inner_only
-    def _():
-        for k in near:
-            up_send(k)
-        for k in near:
-            down_send(k)
-
+    every(last_far, passed)
     up_piece(1, 1).start()
     down_send(1)
     for k in near:
@@ -316,10 +310,17 @@
             state = lax.fori_loop(0, number, step, state)
         return (state[2] / state[1]).astype(BF16)
 
+    for c in later:
+        c.wait()
     for h in range(heads_a):
         res_a = attend(q_a, key_a, val_a, h, depth_a, V_A)
         for j in range(m):
             att[j, :, h * V_A:(h + 1) * V_A] = res_a[j * own:(j + 1) * own]
+    @inner_only
+    def _():
+        for k in near:
+            up_on(k)
+
     for h in range(heads_b):
         res_b = attend(q_b, key_b, val_b, h, depth_b, V_B)
         for j in range(m):
@@ -341,6 +342,12 @@
         return (jnp.dot(rows[k, :, 0:width_a], goa[slot], preferred_element_type=F32)
                 + jnp.dot(rows[k, :, start_b:], gob[slot], preferred_element_type=F32))
 
+    @outer_only
+    def _():
+        for k in near:
+            up_on(k)
+
+    inner_only(lambda: every(2 * quarter, up_on))
     mixed = (jnp.dot(att[t, :, 0:width_a], wo_a[...], preferred_element_type=F32)
              + jnp.dot(att[t, :, start_b:], wo_b[...], preferred_element_type=F32))
     out_a(1, 0).wait_recv()
@@ -396,37 +403,30 @@
     xcopy(0, 2, 2).start()
     xcopy(0, 1, 1).start()
 
+    for k in near:
+        down_send(k)
+
     @outer_only
     def _():
-        for k in near:
-            down_send(k)
         every(first_far, lambda k: down_piece(k, 0).start())
         every(last_far, lambda k: down_piece(k, 0).start())
         if cuts > 1:
             every(first_far, lambda k: down_piece(k, 1).start())
             every(last_far, lambda k: down_piece(k, 1).start())
 
-    for k in near:
-        up_on(k)
-    every(2 * quarter, up_on)
+    @outer_only
+    def _():
+        every(3 * quarter, up_on)
+        every(2 * quarter, up_on)
+
     xcopy(0, 2, 2).wait_recv()
     xcopy(2, 3, 1).start()
-    every(3 * quarter, up_on)
     xrelay()
-
-    @outer_only
-    def _():
-        for k in near:
-            downs_on(k)
-
+    inner_only(lambda: every(3 * quarter, up_on))
     xcopy(4, 6, 2).wait_recv()
     xcopy(6, 7, 1).start()
-
-    @inner_only
-    def _():
-        for k in near:
-            downs_on(k)
-        every(3 * quarter, downs_on)
+    for k in near:
+        downs_on(k)
 
     def columns(k, size):
         return pl.ds(pl.multiple_of((s ^ k) * size, 128), size)
@@ -520,8 +520,8 @@
         every(start + 1, lambda k: down(unit, k, h, cut))
         share(unit, narrow).start()
 
-    def far_on(h):
-        every(2 * quarter, lambda k: down_on(k, h))
+    def far_on(group, h):
+        every(group * quarter, lambda k: down_on(k, h))
 
     down(mine_u, 0, None, wcols)
     down_arrived(1)
@@ -530,29 +530,29 @@
         if k < quarter:
             down_pair(mine_u)(k)
     share(mine_u, full).start()
-    outer_only(lambda: every(3 * quarter, downs_on))
+    inner_only(lambda: far_on(2, 0))
     for k in near:
         if k >= quarter:
             down_pair(next_u)(k)
     share(next_u, full).start()
     scatter(mine_u, full)
-    far_on(0)
     for h in range(cuts):
+        far_on(3, h)
+    outer_only(lambda: far_on(2, 0))
+    far(3, 0)
+    scatter(next_u, full)
+    for h in range(1, cuts):
+        far_on(2, h)
         far(3, h)
-        if h == 0:
-            scatter(next_u, full)
-        else:
-            scatter(far_unit(3, h - 1), narrow)
-    for h in range(1, cuts):
-        far_on(h)
+        scatter(far_unit(3, h - 1), narrow)
     for h in range(cuts):
         far(2, h)
         if h == 0:
             scatter(far_unit(3, cuts - 1), narrow)
-            finish(mine_u, full, 0, None)
-            finish(next_u, full, 1, None)
         else:
             scatter(far_unit(2, h - 1), narrow)
+    finish(mine_u, full, 0, None)
+    finish(next_u, full, 1, None)
     scatter(far_unit(2, cuts - 1), narrow)
     for h in range(cuts):
         finish(far_unit(3, h), narrow, 3, h)
@@ -576,13 +576,9 @@
         lat_direct(k).wait_send()
         sent(k)
     every(first_far, lambda k: lat_direct(k).wait_send())
+    every(last_far, lambda k: lat_direct(k).wait_send())
     every(first_far, sent)
     every(last_far, sent)
-
-    @inner_only
-    def _():
-        every(first_far, lambda k: lat_along(k).wait_send())
-        every(last_far, lambda k: lat_along(k).wait_send())
 
     def settled(k, carry):
         lat_sibling(k).wait_send()
@@ -650,15 +646,17 @@
         V((units, 3, own, group), BF16),
         V(table.shape, F32),
     ]
-    sizes = [n, n, n, n, n, 3, 3, 3, 3, 2 * n, 2 * n, 2 * n, 2 * n, m, m, 16, 16, 24, 24, 5]
+    given = (stream, query_a.T, query_b.T, latent_gain[None], key_gain_a[None], key_gain_b[None],
+             w_key_a.T, w_value_a.T, w_key_b, w_value_b, w_out_a, w_out_b, norm_gain[None])
+    scratch += [V(a.shape, a.dtype) for a in given]
+    sizes = [n, n, n, n, 3, 3, 3, 3, 2 * n, 2 * n, 2 * n, 2 * n, m, m, 16, 16, 24, 24, 18]
     scratch += [dma(k) for k in sizes]
     vmem = pl.BlockSpec(memory_space=V)
     hbm = pl.BlockSpec(memory_space=pl.ANY)
     return pl.pallas_call(
         functools.partial(kernel, n, m),
         out_shape=jax.ShapeDtypeStruct((own, features), BF16),
-        in_specs=[vmem, vmem, vmem, hbm, hbm, hbm, vmem, vmem, vmem, vmem, vmem, vmem, vmem,
-                  vmem, vmem, vmem, hbm, hbm],
+        in_specs=[hbm] * 18,
         out_specs=vmem,
         scratch_shapes=scratch,
         compiler_params=pltpu.CompilerParams(

time: 78.1 us -> 74.3 us (0.951)
  Pallas kernels: 76.3 us -> 72.5 us
    pallas_call x1, Pallas kernels: 76.3 us -> 72.5 us  [body(): pl.pallas_call(functools.partial(kernel, n, m), out_shape=jax.ShapeDtypeS...]
where the time goes in v2:
time: 74.3 us; the launch traced here: 74.2 us
  Pallas kernels  72.5 us (98%)
  local copies, waits for them, and re-layouts  1.67 us (2%)
    pallas_call x1, Pallas kernels, body(): pl.pallas_call(functools.partial(kernel, n, m), out_shape=jax.ShapeDtypeS...  72.5 us
    unnamed x1, local copies, waits for them, and re-layouts  1.67 us

profile of v2, /device:TPU:0, one launch (start us, length us, event | category | flops | bytes accessed | tf_op | source)
XLA Modules:
  0.0 74.2 jit_solution(10916068413531879451)
XLA Ops:
  0.0 72.5 %layer.1 = bf16[64,2048]{1,0:T(8,128)(2,1)} custom-call(bf16[64,2048]{1,0:T(8,128)(2,1)} %stream_h.1, bf16[96,256]{1,0:T(8,128)(2,1)} %bitcast.10, bf16[160,256]{1,0:T(8,128)(2,1)} %bitcast.9, bf16[256,256]{1,0:T(8,128)(2,1)} %latent.1, bf16[32,256]{1,0:T(8,128)(2,1)} %bitcast.13, f32[8,256,32]{2,1,0:T(8,128)} %constant.2.clone.table_h, f32[1,256]{1,0:T(1,128)} %bitcast.15, ...), custom_call_target="tpu_custom_call" | custom-call | tf_op jit(solution)/shard_map/layer/pallas_call | solution.py:656
  72.5 1.7 %copy.20 = bf16[64,2048]{1,0:T(8,128)(2,1)} copy(bf16[64,2048]{1,0:T(8,128)(2,1)} %layer.1) | data formatting | bytes 524288

commit v3 on v2

--- a/solution.py
+++ b/solution.py
@@ -113,32 +113,32 @@
     other = pl.ds(pl.multiple_of((1 - core) * half_rows, 16), half_rows)
 
     def lat_direct(k):
-        return copy(lat.at[0, mine], lat.at[k, mine], lat_s.at[k], lat_r.at[k], s ^ k, t)
+        return copy(lat.at[0, mine], lat.at[k, mine], lat_s.at[0], lat_r.at[k], s ^ k, t)
 
     def lat_across(k):
-        return copy(lat.at[k, mine], lat.at[k + 1, mine], lat_s.at[k + 1], lat_r.at[k + 1], s ^ 1, t)
+        return copy(lat.at[k, mine], lat.at[k + 1, mine], lat_s.at[0], lat_r.at[k + 1], s ^ 1, t)
 
     def lat_sibling(k):
-        return copy(lat.at[k, mine], lat.at[k, mine], latf_s.at[k], latf_r.at[k], s, t ^ 1)
+        return copy(lat.at[k, mine], lat.at[k, mine], latf_s.at[0], latf_r.at[k], s, t ^ 1)
 
     def up_piece(k, r):
         at = pl.ds(r * up_half, up_half)
-        return copy(w_up.at[at, halves(s ^ k)], gup.at[k, at], up_s.at[2 * k + r],
+        return copy(w_up.at[at, halves(s ^ k)], gup.at[k, at], up_s.at[0],
                     up_r.at[2 * k + r], s ^ k, t)
 
     def up_across(k, r):
         at = pl.ds(r * up_half, up_half)
-        return copy(gup.at[k, at], gup.at[k + 1, at], up_s.at[2 * k + 2 + r],
+        return copy(gup.at[k, at], gup.at[k + 1, at], up_s.at[0],
                     up_r.at[2 * k + 2 + r], s ^ 1, t)
 
     def down_piece(k, h):
         at = pl.ds(h * cut, cut)
-        return copy(w_down.at[halves(s ^ k), at], gdown.at[k, :, at], dn_s.at[2 * k + h],
+        return copy(w_down.at[halves(s ^ k), at], gdown.at[k, :, at], dn_s.at[0],
                     dn_r.at[2 * k + h], s ^ k, t)
 
     def down_across(k, h):
         at = pl.ds(h * cut, cut)
-        return copy(gdown.at[k, :, at], gdown.at[k + 1, :, at], dn_s.at[2 * k + 2 + h],
+        return copy(gdown.at[k, :, at], gdown.at[k + 1, :, at], dn_s.at[0],
                     dn_r.at[2 * k + 2 + h], s ^ 1, t)
 
     def up_send(k):
@@ -180,10 +180,10 @@
     up_piece(1, 0).start()
 
     def out_a(k, slot):
-        return copy(wo_a_h, goa.at[slot], oa_s.at[slot], oa_r.at[slot], s, t ^ k)
+        return copy(wo_a_h, goa.at[slot], oa_s.at[0], oa_r.at[slot], s, t ^ k)
 
     def out_b(k, slot):
-        return copy(wo_b_h, gob.at[slot], ob_s.at[slot], ob_r.at[slot], s, t ^ k)
+        return copy(wo_b_h, gob.at[slot], ob_s.at[0], ob_r.at[slot], s, t ^ k)
 
     for k in (2, 1):
         out_a(k, k - 1).start()
@@ -248,7 +248,7 @@
         lat_direct(k).wait_recv()
 
     def joined(k):
-        copy(lat.at[k, other], lat.at[k, other], latf_s.at[k], latf_r.at[k], s, t ^ 1).wait_recv()
+        copy(lat.at[k, other], lat.at[k, other], latf_s.at[0], latf_r.at[k], s, t ^ 1).wait_recv()
         make_block(k)
 
     def passed(k):
@@ -327,16 +327,16 @@
             att[j, :, start_b + h * V_B:start_b + (h + 1) * V_B] = res_b[j * own:(j + 1) * own]
 
     def row_copy(k):
-        return copy(att.at[t ^ k], rows.at[k], at_s.at[k], at_r.at[k], s, t ^ k)
+        return copy(att.at[t ^ k], rows.at[k], at_s.at[0], at_r.at[k], s, t ^ k)
 
     for k in (2, 3, 1):
         row_copy(k).start()
 
     def out_on_a():
-        return copy(goa.at[1], goa.at[2], oa_s.at[2], oa_r.at[2], s, t ^ 1)
+        return copy(goa.at[1], goa.at[2], oa_s.at[0], oa_r.at[2], s, t ^ 1)
 
     def out_on_b():
-        return copy(gob.at[1], gob.at[2], ob_s.at[2], ob_r.at[2], s, t ^ 1)
+        return copy(gob.at[1], gob.at[2], ob_s.at[0], ob_r.at[2], s, t ^ 1)
 
     def project(k, slot):
         return (jnp.dot(rows[k, :, 0:width_a], goa[slot], preferred_element_type=F32)
@@ -379,7 +379,7 @@
         def __init__(self, src, dst, code):
             self.parts = [
                 copy(x.at[pl.ds(src * own + i * bit, bit)], x.at[pl.ds(dst * own + i * bit, bit)],
-                     x_s.at[2 * dst + i], x_r.at[2 * dst + i], *peer(code)) for i in range(2)]
+                     x_s.at[0], x_r.at[2 * dst + i], *peer(code)) for i in range(2)]
 
         def start(self):
             for c in self.parts:
@@ -479,12 +479,12 @@
 
     def share(unit, width):
         return copy(odd.at[unit, :, :, 0:width], sib.at[unit, :, :, 0:width],
-                    rs_s.at[4 * unit], rs_r.at[4 * unit], s, t ^ 1)
+                    rs_s.at[0], rs_r.at[4 * unit], s, t ^ 1)
 
     def deliver(unit, width, i):
         _, sp, tp = places[i]
         return copy(part.at[unit, i, :, 0:width], land.at[unit, i, :, 0:width],
-                    rs_s.at[4 * unit + 1 + i], rs_r.at[4 * unit + 1 + i], sp, tp)
+                    rs_s.at[0], rs_r.at[4 * unit + 1 + i], sp, tp)
 
     def scatter(unit, width):
         share(unit, width).wait_recv()
@@ -559,48 +559,18 @@
     for h in range(cuts):
         finish(far_unit(2, h), narrow, 2, h)
 
-    lat_direct(1).wait_send()
-    up_piece(1, 0).wait_send()
-    up_piece(1, 1).wait_send()
-
-    def sent(k):
-        lat_across(k).wait_send()
-        for r in range(2):
-            up_piece(k, r).wait_send()
-            up_across(k, r).wait_send()
-        for h in range(cuts):
-            down_piece(k, h).wait_send()
-            down_across(k, h).wait_send()
-
-    for k in near:
-        lat_direct(k).wait_send()
-        sent(k)
-    every(first_far, lambda k: lat_direct(k).wait_send())
-    every(last_far, lambda k: lat_direct(k).wait_send())
-    every(first_far, sent)
-    every(last_far, sent)
-
-    def settled(k, carry):
-        lat_sibling(k).wait_send()
-        return carry
-
-    lax.fori_loop(1, n, settled, 0)
-    for h in range(cuts):
-        down_piece(1, h).wait_send()
-    for k in (1, 2):
-        out_a(k, k - 1).wait_send()
-        out_b(k, k - 1).wait_send()
-    out_on_a().wait_send()
-    out_on_b().wait_send()
-    for k in range(1, m):
-        row_copy(k).wait_send()
-    for src, dst, code in ((0, 4, 4), (0, 2, 2), (0, 1, 1), (2, 3, 1), (4, 6, 2), (4, 5, 1), (6, 7, 1)):
-        xcopy(src, dst, code).wait_send()
-    units = [(0, full), (1, full)] + [(2 + i, narrow) for i in range(2 * cuts)]
-    for unit, width in units:
-        share(unit, width).wait_send()
-        for i in range(3):
-            deliver(unit, width, i).wait_send()
+    def drained(ref, sem):
+        copy(ref, ref, sem.at[0], sem.at[0], s, t ^ 1).wait_send()
+
+    drained(lat.at[pl.ds(1, n - 1), mine], lat_s)
+    drained(lat.at[pl.ds(1, n - 1), mine], latf_s)
+    drained(gup.at[pl.ds(1, n - 1)], up_s)
+    drained(gdown.at[pl.ds(1, n - 1)], dn_s)
+    drained(goa, oa_s)
+    drained(gob, ob_s)
+    drained(rows.at[pl.ds(1, m - 1)], at_s)
+    drained(x.at[pl.ds(own, 7 * own)], x_s)
+    drained(x.at[pl.ds(0, 7 * own)], rs_s)
 
 
 def body(n, m, stream, query_a, query_b, latent, rotary_key, latent_gain, key_gain_a, key_gain_b,
@@ -649,7 +619,7 @@
     given = (stream, query_a.T, query_b.T, latent_gain[None], key_gain_a[None], key_gain_b[None],
              w_key_a.T, w_value_a.T, w_key_b, w_value_b, w_out_a, w_out_b, norm_gain[None])
     scratch += [V(a.shape, a.dtype) for a in given]
-    sizes = [n, n, n, n, 3, 3, 3, 3, 2 * n, 2 * n, 2 * n, 2 * n, m, m, 16, 16, 24, 24, 18]
+    sizes = [1, n, 1, n, 1, 3, 1, 3, 1, 2 * n, 1, 2 * n, 1, m, 1, 16, 1, 24, 18]
     scratch += [dma(k) for k in sizes]
     vmem = pl.BlockSpec(memory_space=V)
     hbm = pl.BlockSpec(memory_space=pl.ANY)

time: 74.3 us -> 73.4 us (0.988)
  Pallas kernels: 72.5 us -> 71.5 us
    pallas_call x1, Pallas kernels: 72.5 us -> 71.5 us  [body(): pl.pallas_call(functools.partial(kernel, n, m), out_shape=jax.ShapeDtypeS...]
where the time goes in v3:
time: 73.4 us; the launch traced here: 73.2 us
  Pallas kernels  71.5 us (97%)
  local copies, waits for them, and re-layouts  1.67 us (2%)
    pallas_call x1, Pallas kernels, body(): pl.pallas_call(functools.partial(kernel, n, m), out_shape=jax.ShapeDtypeS...  71.5 us
    unnamed x1, local copies, waits for them, and re-layouts  1.67 us

profile of v3, /device:TPU:0, one launch (start us, length us, event | category | flops | bytes accessed | tf_op | source)
XLA Modules:
  0.0 73.2 jit_solution(9885270495677111923)
XLA Ops:
  0.0 71.5 %layer.1 = bf16[64,2048]{1,0:T(8,128)(2,1)} custom-call(bf16[64,2048]{1,0:T(8,128)(2,1)} %stream_h.1, bf16[96,256]{1,0:T(8,128)(2,1)} %bitcast.10, bf16[160,256]{1,0:T(8,128)(2,1)} %bitcast.9, bf16[256,256]{1,0:T(8,128)(2,1)} %latent.1, bf16[32,256]{1,0:T(8,128)(2,1)} %bitcast.13, f32[8,256,32]{2,1,0:T(8,128)} %constant.2.clone.table_h, f32[1,256]{1,0:T(1,128)} %bitcast.15, ...), custom_call_target="tpu_custom_call" | custom-call | tf_op jit(solution)/shard_map/layer/pallas_call | solution.py:626
  71.5 1.7 %copy.20 = bf16[64,2048]{1,0:T(8,128)(2,1)} copy(bf16[64,2048]{1,0:T(8,128)(2,1)} %layer.1) | data formatting | bytes 524288

commit v4 on v3

--- a/solution.py
+++ b/solution.py
@@ -18,6 +18,19 @@
 THETA = 10000.0
 F32 = jnp.float32
 BF16 = jnp.bfloat16
+
+
+class Several:
+    def __init__(self, parts):
+        self.parts = parts
+
+    def start(self):
+        for c in self.parts:
+            c.start()
+
+    def wait_recv(self):
+        for c in self.parts:
+            c.wait_recv()
 
 
 def kernel(
@@ -131,15 +144,23 @@
         return copy(gup.at[k, at], gup.at[k + 1, at], up_s.at[0],
                     up_r.at[2 * k + 2 + r], s ^ 1, t)
 
+    def down_parts(k, h):
+        at = pl.ds(h * cut, cut)
+        size = hidden // (1 + h)
+        for r in range(1 + h):
+            yield (pl.ds(pl.multiple_of(((s ^ k) // 2) % 2 * hidden + r * size, 128), size),
+                   pl.ds(r * size, size), at, h + r)
+
     def down_piece(k, h):
-        at = pl.ds(h * cut, cut)
-        return copy(w_down.at[halves(s ^ k), at], gdown.at[k, :, at], dn_s.at[0],
-                    dn_r.at[2 * k + h], s ^ k, t)
+        return Several([
+            copy(w_down.at[src, at], gdown.at[k, dst, at], dn_s.at[0], dn_r.at[3 * k + i], s ^ k, t)
+            for src, dst, at, i in down_parts(k, h)])
 
     def down_across(k, h):
-        at = pl.ds(h * cut, cut)
-        return copy(gdown.at[k, :, at], gdown.at[k + 1, :, at], dn_s.at[0],
-                    dn_r.at[2 * k + 2 + h], s ^ 1, t)
+        return Several([
+            copy(gdown.at[k, dst, at], gdown.at[k + 1, dst, at], dn_s.at[0],
+                 dn_r.at[3 * k + 3 + i], s ^ 1, t)
+            for src, dst, at, i in down_parts(k, h)])
 
     def up_send(k):
         for r in range(2):
@@ -159,8 +180,9 @@
             up_piece(k, r).wait_recv()
 
     def down_on(k, h):
-        down_piece(k, h).wait_recv()
-        down_across(k, h).start()
+        for come, go in zip(down_piece(k, h).parts, down_across(k, h).parts):
+            come.wait_recv()
+            go.start()
 
     def downs_on(k):
         for h in range(cuts):
@@ -193,8 +215,9 @@
     def _():
         every(last_far, up_send)
         every(first_far, up_send)
-        every(first_far, down_send)
-        every(last_far, down_send)
+        for h in range(cuts):
+            every(last_far, lambda k: down_piece(k, h).start())
+            every(first_far, lambda k: down_piece(k, h).start())
         for k in near:
             up_send(k)
 
@@ -375,23 +398,10 @@
 
     bit = own // 2
 
-    class xcopy:
-        def __init__(self, src, dst, code):
-            self.parts = [
-                copy(x.at[pl.ds(src * own + i * bit, bit)], x.at[pl.ds(dst * own + i * bit, bit)],
-                     x_s.at[0], x_r.at[2 * dst + i], *peer(code)) for i in range(2)]
-
-        def start(self):
-            for c in self.parts:
-                c.start()
-
-        def wait_recv(self):
-            for c in self.parts:
-                c.wait_recv()
-
-        def wait_send(self):
-            for c in self.parts:
-                c.wait_send()
+    def xcopy(src, dst, code):
+        return Several([
+            copy(x.at[pl.ds(src * own + i * bit, bit)], x.at[pl.ds(dst * own + i * bit, bit)],
+                 x_s.at[0], x_r.at[2 * dst + i], *peer(code)) for i in range(2)])
 
     def xrelay():
         for i in range(2):
@@ -408,11 +418,9 @@
 
     @outer_only
     def _():
-        every(first_far, lambda k: down_piece(k, 0).start())
-        every(last_far, lambda k: down_piece(k, 0).start())
-        if cuts > 1:
-            every(first_far, lambda k: down_piece(k, 1).start())
-            every(last_far, lambda k: down_piece(k, 1).start())
+        for h in range(cuts):
+            every(first_far, lambda k: down_piece(k, h).start())
+            every(last_far, lambda k: down_piece(k, h).start())
 
     @outer_only
     def _():
@@ -530,34 +538,43 @@
         if k < quarter:
             down_pair(mine_u)(k)
     share(mine_u, full).start()
-    inner_only(lambda: far_on(2, 0))
+    one, two = 2 + inner, 3 - inner
+    outer_only(lambda: far_on(one, 0))
+    far_on(two, 0)
     for k in near:
         if k >= quarter:
             down_pair(next_u)(k)
     share(next_u, full).start()
     scatter(mine_u, full)
-    for h in range(cuts):
-        far_on(3, h)
-    outer_only(lambda: far_on(2, 0))
+
+    @inner_only
+    def _():
+        if cuts > 1:
+            far_on(two, 1)
+        far_on(one, 0)
+
+    far(2, 0)
+    if cuts > 1:
+        outer_only(lambda: far_on(two, 1))
+    scatter(next_u, full)
     far(3, 0)
-    scatter(next_u, full)
-    for h in range(1, cuts):
-        far_on(2, h)
-        far(3, h)
-        scatter(far_unit(3, h - 1), narrow)
-    for h in range(cuts):
-        far(2, h)
-        if h == 0:
-            scatter(far_unit(3, cuts - 1), narrow)
-        else:
-            scatter(far_unit(2, h - 1), narrow)
-    finish(mine_u, full, 0, None)
-    finish(next_u, full, 1, None)
-    scatter(far_unit(2, cuts - 1), narrow)
-    for h in range(cuts):
-        finish(far_unit(3, h), narrow, 3, h)
-    for h in range(cuts):
-        finish(far_unit(2, h), narrow, 2, h)
+    scatter(far_unit(2, 0), narrow)
+    if cuts > 1:
+        far_on(one, 1)
+        scatter(far_unit(3, 0), narrow)
+        far(two, 1)
+        scatter(far_unit(two, 1), narrow)
+        far(one, 1)
+        scatter(far_unit(one, 1), narrow)
+        finish(mine_u, full, 0, None)
+        finish(next_u, full, 1, None)
+    else:
+        scatter(far_unit(3, 0), narrow)
+        finish(mine_u, full, 0, None)
+        finish(next_u, full, 1, None)
+    for group in (two, one):
+        for h in range(cuts):
+            finish(far_unit(group, h), narrow, group, h)
 
     def drained(ref, sem):
         copy(ref, ref, sem.at[0], sem.at[0], s, t ^ 1).wait_send()
@@ -619,7 +636,7 @@
     given = (stream, query_a.T, query_b.T, latent_gain[None], key_gain_a[None], key_gain_b[None],
              w_key_a.T, w_value_a.T, w_key_b, w_value_b, w_out_a, w_out_b, norm_gain[None])
     scratch += [V(a.shape, a.dtype) for a in given]
-    sizes = [1, n, 1, n, 1, 3, 1, 3, 1, 2 * n, 1, 2 * n, 1, m, 1, 16, 1, 24, 18]
+    sizes = [1, n, 1, n, 1, 3, 1, 3, 1, 2 * n, 1, 3 * n, 1, m, 1, 16, 1, 24, 18]
     scratch += [dma(k) for k in sizes]
     vmem = pl.BlockSpec(memory_space=V)
     hbm = pl.BlockSpec(memory_space=pl.ANY)

time: 73.4 us -> 71.4 us (0.973)
  Pallas kernels: 71.5 us -> 69.6 us
    pallas_call x1, Pallas kernels: 71.5 us -> 69.6 us  [body(): pl.pallas_call(functools.partial(kernel, n, m), out_shape=jax.ShapeDtypeS...]
where the time goes in v4:
time: 71.4 us; the launch traced here: 71.2 us
  Pallas kernels  69.6 us (97%)
  local copies, waits for them, and re-layouts  1.67 us (2%)
    pallas_call x1, Pallas kernels, body(): pl.pallas_call(functools.partial(kernel, n, m), out_shape=jax.ShapeDtypeS...  69.6 us
    unnamed x1, local copies, waits for them, and re-layouts  1.67 us

profile of v4, /device:TPU:0, one launch (start us, length us, event | category | flops | bytes accessed | tf_op | source)
XLA Modules:
  0.0 71.2 jit_solution(15571342443599309089)
XLA Ops:
  0.0 69.6 %layer.1 = bf16[64,2048]{1,0:T(8,128)(2,1)} custom-call(bf16[64,2048]{1,0:T(8,128)(2,1)} %stream_h.1, bf16[96,256]{1,0:T(8,128)(2,1)} %bitcast.10, bf16[160,256]{1,0:T(8,128)(2,1)} %bitcast.9, bf16[256,256]{1,0:T(8,128)(2,1)} %latent.1, bf16[32,256]{1,0:T(8,128)(2,1)} %bitcast.13, f32[8,256,32]{2,1,0:T(8,128)} %constant.2.clone.table_h, f32[1,256]{1,0:T(1,128)} %bitcast.15, ...), custom_call_target="tpu_custom_call" | custom-call | tf_op jit(solution)/shard_map/layer/pallas_call | solution.py:643
  69.6 1.7 %copy.20 = bf16[64,2048]{1,0:T(8,128)(2,1)} copy(bf16[64,2048]{1,0:T(8,128)(2,1)} %layer.1) | data formatting | bytes 524288
